TPU v7x, 32 devices: a whole 2x2x4 slice. The times are simulated.
32 devices in a mesh: sp: 8 (over z, y), tp: 4 (over x, core).
Axes of the slice: x: 2, y: 2, z: 4, core: 2. Of those that a mesh axis runs over, the one named last changes fastest.
Arguments:
- queries: bfloat16 [4096, 2048], P('sp', 'tp'), may hold values from -8 to 8
- keys: bfloat16 [4096, 512], P('sp', 'tp'), may hold values from -8 to 8
- values: bfloat16 [4096, 512], P('sp', 'tp'), may hold values from -6 to 6
- q_gain: float32 [128], replicated, may hold values from 0.1 to 5.8
- k_gain: float32 [128], replicated, may hold values from 0.1 to 5.8
- out_weight: bfloat16 [2048, 2048], replicated, may hold values from -0.125 to 0.125
- out_gain: float32 [2048], replicated, may hold values from 0.1 to 1.9
- residual_in: bfloat16 [4096, 2048], P(('sp', 'tp')), may hold values from -6 to 6
- mlp_gain: float32 [2048], replicated, may hold values from 0.1 to 1.9
- gate_weight: bfloat16 [2048, 5632], P('sp', 'tp'), may hold values from -0.125 to 0.125
- up_weight: bfloat16 [2048, 5632], P('sp', 'tp'), may hold values from -0.125 to 0.125
- down_weight: bfloat16 [5632, 2048], P('tp', 'sp'), may hold values from -0.078125 to 0.078125
- final_gain: float32 [2048], replicated, may hold values from 0.1 to 1.9
Outputs:
- layer_out: bfloat16 [4096, 2048], P(('sp', 'tp'))
All inputs are finite; a program needn't handle non-finite values.
Results may differ from a plain program's by a relative error of at most 0.015.
The roundings to bfloat16 on the way count: a program that leaves them out, or rounds other values in their place, can miss the bound.
Values may be sent and summed in bfloat16 or wider, within the bound.
A program may use at most 128 MiB of HBM per device.

v0:
```python
import math
import jax
import jax.numpy as jnp
from jax import lax
from jax.sharding import PartitionSpec as P

GRID_W = 64


def rms_scale(matrix):
    return matrix * lax.rsqrt(jnp.mean(matrix * matrix, axis=-1, keepdims=True) + 1e-06)


def rotary(matrix, positions):
    quarter = matrix.shape[-1] // 4
    freqs = 10000.0 ** (-jnp.arange(quarter, dtype=jnp.float32) / quarter)
    grid = jnp.stack([positions // GRID_W, positions % GRID_W], axis=-1).astype(jnp.float32)
    angle = grid[:, :, None] * freqs
    cosine = jnp.cos(angle)[:, None]
    sine = jnp.sin(angle)[:, None]
    parts = matrix.reshape(matrix.shape[:-1] + (2, 2, quarter))
    first = parts[..., 0, :]
    second = parts[..., 1, :]
    turned = jnp.stack([first * cosine - second * sine, second * cosine + first * sine], axis=-2)
    return turned.reshape(matrix.shape)


def on_device(
    queries,
    keys,
    values,
    q_gain,
    k_gain,
    out_weight,
    out_gain,
    residual_in,
    mlp_gain,
    gate_weight,
    up_weight,
    down_weight,
    final_gain,
):
    tok_rows = queries.shape[0]
    head_size = q_gain.shape[0]
    q_heads = queries.shape[1] // head_size
    kv_heads = keys.shape[1] // head_size
    group_size = q_heads // kv_heads
    positions = lax.axis_index("sp") * tok_rows + jnp.arange(tok_rows, dtype=jnp.int32)
    query_rot = rotary(
        rms_scale(queries.reshape(tok_rows, q_heads, head_size).astype(jnp.float32)) * q_gain,
        positions,
    ).astype(jnp.bfloat16)
    key_rot = rotary(
        rms_scale(keys.reshape(tok_rows, kv_heads, head_size).astype(jnp.float32)) * k_gain,
        positions,
    ).astype(jnp.bfloat16)
    key_flat = key_rot.reshape(tok_rows, kv_heads * head_size)
    grouped = query_rot.reshape(tok_rows, kv_heads, group_size, head_size)
    score_scale = head_size ** (-0.5)
    key_all, value_all = (
        lax.all_gather(key_flat, "sp", axis=0, tiled=True),
        lax.all_gather(values, "sp", axis=0, tiled=True),
    )
    total_rows = key_all.shape[0]
    span = math.gcd(total_rows, 1024)
    key_blocks = key_all.reshape(total_rows // span, span, kv_heads, head_size)
    value_blocks = value_all.reshape(total_rows // span, span, kv_heads, head_size)

    def step(run_state, blocks):
        highest, weight_sum, accum = run_state
        key_block, value_block = blocks
        scores = (
            jnp.einsum("qcgd,kcd->cgqk", grouped, key_block, preferred_element_type=jnp.float32)
            * score_scale
        )
        new_high = jnp.maximum(highest, jnp.max(scores, axis=-1))
        factor = jnp.exp(highest - new_high)
        exp_scores = jnp.exp(scores - new_high[..., None])
        weight_sum = weight_sum * factor + jnp.sum(exp_scores, axis=-1)
        accum = accum * factor[..., None] + jnp.einsum(
            "cgqk,kcd->cgqd",
            exp_scores.astype(jnp.bfloat16),
            value_block,
            preferred_element_type=jnp.float32,
        )
        return ((new_high, weight_sum, accum), None)

    start_state = (
        jnp.full((kv_heads, group_size, tok_rows), -1e30, jnp.float32),
        jnp.zeros((kv_heads, group_size, tok_rows), jnp.float32),
        jnp.zeros((kv_heads, group_size, tok_rows, head_size), jnp.float32),
    )
    final_state, unused = lax.scan(step, start_state, (key_blocks, value_blocks))
    highest, weight_sum, accum = final_state
    attended = (
        jnp.transpose(accum / weight_sum[..., None], (2, 0, 1, 3))
        .reshape(tok_rows, q_heads * head_size)
        .astype(jnp.bfloat16)
    )
    head_rows = lax.all_to_all(attended, "tp", split_axis=0, concat_axis=1, tiled=True)
    projected = jnp.dot(head_rows, out_weight, preferred_element_type=jnp.float32)
    mid_stream = (residual_in.astype(jnp.float32) + out_gain * rms_scale(projected)).astype(
        jnp.bfloat16
    )
    normed = (mlp_gain * rms_scale(mid_stream.astype(jnp.float32))).astype(jnp.bfloat16)
    mixer_in = lax.all_gather(normed, "tp", axis=0, tiled=True)
    gate_proj = jnp.dot(
        mixer_in,
        lax.all_gather(gate_weight, "sp", axis=0, tiled=True),
        preferred_element_type=jnp.float32,
    )
    up_proj = jnp.dot(
        mixer_in,
        lax.all_gather(up_weight, "sp", axis=0, tiled=True),
        preferred_element_type=jnp.float32,
    )
    down_full = lax.all_gather(down_weight, "sp", axis=1, tiled=True)
    hidden = (jax.nn.silu(gate_proj) * up_proj).astype(jnp.bfloat16)
    mlp_branch = lax.psum_scatter(
        jnp.dot(hidden, down_full, preferred_element_type=jnp.float32).astype(jnp.bfloat16),
        "tp",
        scatter_dimension=0,
        tiled=True,
    ).astype(jnp.float32)
    return (mid_stream.astype(jnp.float32) + final_gain * rms_scale(mlp_branch)).astype(
        jnp.bfloat16
    )


def solution(mesh):
    return jax.shard_map(
        on_device,
        mesh=mesh,
        in_specs=(
            P("sp", "tp"),
            P("sp", "tp"),
            P("sp", "tp"),
            P(),
            P(),
            P(),
            P(),
            P(("sp", "tp"), None),
            P(),
            P("sp", "tp"),
            P("sp", "tp"),
            P("tp", "sp"),
            P(),
        ),
        out_specs=P(("sp", "tp"), None),
        check_vma=False,
    )
```

profile of v0, /device:TPU:0, one launch (start us, length us, event | category | flops | bytes accessed | tf_op | source)
XLA Modules:
  0.0 513.3 jit_solution(11249257965567632647)
XLA Ops:
  6.6 1.0 copy.17
  7.7 0.7 fusion.33
  8.4 0.6 fusion.39
  9.0 0.7 pad_maximum_fusion.1
  9.7 0.7 all-gather.9.cloned.1.call-update
  10.5 1.3 copy.18
  11.8 0.7 mul.257
  12.7 0.5 multiply_cosine_fusion
  13.6 0.3 copy.20
  13.9 38.1 %all-gather.7.cloned.1.call-done = bf16[4096,128]{0,1:T(8,128)(2,1)} async-done(((bf16[512,128]{0,1:T(8,128)(2,1)}), bf16[4096,128]{0,1:T(8,128)(2,1)}) %all-gather.7.cloned.1.call-update) | async-done | bytes 1048592 | tf_op jit(solution)/shard_map/all_gather | solution.py:61
  52.0 1.6 copy.24
  53.6 39.8 %all-gather.9.cloned.1.call-done = bf16[4096,128]{1,0:T(8,128)(2,1)} async-done(((bf16[512,128]{1,0:T(8,128)(2,1)}), bf16[4096,128]{1,0:T(8,128)(2,1)}) %all-gather.9.cloned.1.call-update) | async-done | bytes 1048592 | tf_op jit(solution)/shard_map/all_gather | solution.py:62
  93.4 47.3 %while.15 = (s32[]{:T(128)}, f32[1,4,512]{2,1,0:T(4,128)S(1)}, f32[1,4,512]{2,1,0:T(4,128)S(1)}, f32[1,4,512,128]{3,2,1,0:T(8,128)S(1)}, bf16[4,1024,1,128]{3,1,...) while((s32[]{:T(128)}, f32[1,4,512]{2,1,0:T(4,128)S(1)}, ...), condition=%wide.region_5.6_spmd.clone, body=%wide.region_2.5_spmd.clone.sunk | while | flops 1091317760 | bytes 61997704 | solution.py:93
  93.4 4.5 bitcast_reduce_fusion.3
  97.9 4.6 fusion.60
  102.5 1.3 copy-done
  103.8 1.4 fusion.59
  105.2 4.5 bitcast_reduce_fusion.3
  109.7 4.6 fusion.60
  114.3 1.3 copy-done
  115.6 1.4 fusion.59
  117.0 4.5 bitcast_reduce_fusion.3
  121.5 4.6 fusion.60
  126.1 1.3 copy-done
  127.4 1.4 fusion.59
  128.9 4.5 bitcast_reduce_fusion.3
  133.4 4.6 fusion.60
  138.0 1.3 copy-done
  139.3 1.4 fusion.59
  140.7 0.3 fusion.31
  141.0 0.4 copy.21
  141.7 11.4 %all_to_all.16 = bf16[4,128,512]{2,1,0:T(8,128)(2,1)S(1)} all-to-all(bf16[4,128,512]{2,1,0:T(8,128)(2,1)S(1)} %convert_element_type.88), channel_id=1, replica_groups=mesh['sp'=8,'tp'=4] {'tp'}, dimensions={0} | all-to-all | bytes 1048576 | tf_op jit(solution)/shard_map/all_to_all | solution.py:100
  153.0 0.3 copy.22
  153.3 4.8 multiply_reduce_fusion
  158.1 0.4 fusion.27
  158.5 1.0 fusion.29
  159.6 0.5 all-gather.13.cloned.1.call-update
  160.2 0.5 all-gather.15.cloned.1.call-update
  160.8 0.5 all-gather.17.cloned.1.call-update
  161.5 18.5 %all-gather.11.cloned.1.call-done = bf16[512,2048]{1,0:T(8,128)(2,1)} async-done(((bf16[128,2048]{1,0:T(8,128)(2,1)}), bf16[512,2048]{1,0:T(8,128)(2,1)}) %all-gather.11.cloned.1.call-update) | async-done | bytes 2097168 | tf_op jit(solution)/shard_map/all_gather | solution.py:106
  180.1 94.4 %all-gather.13.cloned.1.call-done = bf16[2048,1408]{1,0:T(8,128)(2,1)} async-done(((bf16[256,1408]{1,0:T(8,128)(2,1)}), bf16[2048,1408]{1,0:T(8,128)(2,1)}) %all-gather.13.cloned.1.call-update) | async-done | bytes 5767184 | tf_op jit(solution)/shard_map/all_gather | solution.py:109
  274.4 8.2 %fusion.43 = f32[512,1408]{1,0:T(8,128)} fusion(bf16[512,2048]{1,0:T(8,128)(2,1)} %all-gather.11.cloned.1.call-done, bf16[2048,1408]{1,0:T(8,128)(2,1)} %all-gather.13.cloned.1.call-done), kind=kOutput, calls=%fused_computation.81 | convolution fusion | flops 2952790016 | bytes 10747904 | tf_op jit(solution)/shard_map/dot_general | solution.py:107
  282.7 84.3 %all-gather.15.cloned.1.call-done = bf16[2048,1408]{1,0:T(8,128)(2,1)} async-done(((bf16[256,1408]{1,0:T(8,128)(2,1)}), bf16[2048,1408]{1,0:T(8,128)(2,1)}) %all-gather.15.cloned.1.call-update) | async-done | bytes 5767184 | tf_op jit(solution)/shard_map/all_gather | solution.py:114
  367.0 93.2 %all-gather.17.cloned.1.call-done = bf16[1408,2048]{1,0:T(8,128)(2,1)} async-done(((bf16[1408,256]{1,0:T(8,128)(2,1)}), bf16[1408,2048]{1,0:T(8,128)(2,1)}) %all-gather.17.cloned.1.call-update) | async-done | bytes 5767184 | tf_op jit(solution)/shard_map/all_gather | solution.py:117
  460.2 13.3 %convolution_convert_fusion = bf16[512,2048]{1,0:T(8,128)(2,1)} fusion(bf16[1408,2048]{1,0:T(8,128)(2,1)} %all-gather.17.cloned.1.call-done, bf16[512,2048]{1,0:T(8,128)(2,1)S(1)} %copy-done.5, bf16[2048,1408]{1,0:T(8,128)(2,1)} %all-gather.15.cloned.1.call-done, f32[512,1408]{1,0:T(8,128)} %fusion.43), kind=kOutput, calls=%fused_computation.28 | convolution fusion | flops 5910953984 | bytes 18612224 | tf_op jit(solution)/shard_map/dot_general | solution.py:120
  473.6 29.5 %reduce-scatter.2.cloned.1.call-done = bf16[128,2048]{1,0:T(8,128)(2,1)} async-done(((bf16[512,2048]{1,0:T(8,128)(2,1)}), bf16[128,2048]{1,0:T(8,128)(2,1)}) %reduce-scatter.2.cloned.1.call-update) | async-done | bytes 524304 | tf_op jit(solution)/shard_map/reduce_scatter | solution.py:119
  503.1 1.2 fusion.25
  504.3 2.1 fusion.30
  (53 shorter events, 1.5 us)
Async XLA Ops:
  6.5 45.4 %all-gather.7.cloned.1.call-start = ((), (), s32[]{:S(2)}) async-start(), calls=%async_computation.2 | async-start | bytes 1179648 | tf_op jit(solution)/shard_map/all_gather | solution.py:61
  9.7 83.7 %all-gather.9.cloned.1.call-start = ((), (), s32[]{:S(2)}) async-start(), calls=%async_computation.3 | async-start | bytes 1179648 | tf_op jit(solution)/shard_map/all_gather | solution.py:62
  10.4 169.6 %all-gather.11.cloned.1.call-start = ((), (), s32[]{:S(2)}) async-start(), calls=%async_computation.4 | async-start | bytes 2621440 | tf_op jit(solution)/shard_map/all_gather | solution.py:106
  97.9 5.9 %copy-start = (f32[1024,512,4]{1,0,2:T(8,128)S(1)}, f32[1024,512,4]{1,0,2:T(8,128)}, u32[]{:S(2)}) copy-start(f32[1024,512,4]{1,0,2:T(8,128)} %get-tuple-element.155) | copy-start | bytes 25165828 | tf_op jit(solution)/shard_map/while
  109.7 5.9 %copy-start = (f32[1024,512,4]{1,0,2:T(8,128)S(1)}, f32[1024,512,4]{1,0,2:T(8,128)}, u32[]{:S(2)}) copy-start(f32[1024,512,4]{1,0,2:T(8,128)} %get-tuple-element.155) | copy-start | bytes 25165828 | tf_op jit(solution)/shard_map/while
  121.5 5.9 %copy-start = (f32[1024,512,4]{1,0,2:T(8,128)S(1)}, f32[1024,512,4]{1,0,2:T(8,128)}, u32[]{:S(2)}) copy-start(f32[1024,512,4]{1,0,2:T(8,128)} %get-tuple-element.155) | copy-start | bytes 25165828 | tf_op jit(solution)/shard_map/while
  133.3 5.9 %copy-start = (f32[1024,512,4]{1,0,2:T(8,128)S(1)}, f32[1024,512,4]{1,0,2:T(8,128)}, u32[]{:S(2)}) copy-start(f32[1024,512,4]{1,0,2:T(8,128)} %get-tuple-element.155) | copy-start | bytes 25165828 | tf_op jit(solution)/shard_map/while
  153.3 4.8 copy-start.1
  153.3 4.8 copy-start.2
  153.3 5.2 %copy-start.3 = (f32[2048]{0:T(1024)S(1)}, f32[2048]{0:T(1024)}, u32[]{:S(2)}) copy-start(f32[2048]{0:T(1024)} %param.23) | copy-start | bytes 24580
  159.5 114.9 %all-gather.13.cloned.1.call-start = ((), (), s32[]{:S(2)}) async-start(), calls=%async_computation.5 | async-start | bytes 6488064 | tf_op jit(solution)/shard_map/all_gather | solution.py:109
  160.1 206.9 %all-gather.15.cloned.1.call-start = ((), (), s32[]{:S(2)}) async-start(), calls=%async_computation.6 | async-start | bytes 6488064 | tf_op jit(solution)/shard_map/all_gather | solution.py:114
  160.7 299.5 %all-gather.17.cloned.1.call-start = ((), (), s32[]{:S(2)}) async-start(), calls=%async_computation.7 | async-start | bytes 6488064 | tf_op jit(solution)/shard_map/all_gather | solution.py:117
  161.3 341.8 %reduce-scatter.2.cloned.1.call-start = ((), (), s32[]{:S(2)}) async-start(), calls=%async_computation.8 | async-start | bytes 2621440 | tf_op jit(solution)/shard_map/reduce_scatter | solution.py:119
  180.1 280.2 %copy-start.5 = (bf16[512,2048]{1,0:T(8,128)(2,1)S(1)}, bf16[512,2048]{1,0:T(8,128)(2,1)}, u32[]{:S(2)}) copy-start(bf16[512,2048]{1,0:T(8,128)(2,1)} %all-gather.11.cloned.1.call-done) | copy-start | bytes 6291460
  282.7 221.7 %copy-start.4 = (f32[2048]{0:T(1024)S(1)}, f32[2048]{0:T(1024)}, u32[]{:S(2)}) copy-start(f32[2048]{0:T(1024)} %param.27) | copy-start | bytes 24580
Sparse Core Ops, SparseCore 0:
  9.8 42.1 all-gather.6
  54.1 39.2 all-gather.8
  159.7 20.3 all-gather.10
  182.1 92.3 all-gather.12
  276.5 90.4 all-gather.14
  368.9 91.2 all-gather.16
  473.7 29.3 reduce-scatter.1
where the time goes:
time: 514 us; the launch traced here: 513 us
  waiting for transfers between devices  400 us (78%)
  matrix products  62.7 us (12%)
  other arithmetic  13.9 us (3%)
  between operations  13.7 us (3%)
  blocking collectives  11.4 us (2%)
  local copies, waits for them, and re-layouts  11 us (2%)
    all_gather x1, waiting for transfers between devices, on_device(): lax.all_gather(gate_weight, 'sp', axis=0, tiled=True)  94.4 us
    all_gather x1, waiting for transfers between devices, on_device(): down_full = lax.all_gather(down_weight, 'sp', axis=1, tiled=True)  93.2 us
    all_gather x1, waiting for transfers between devices, on_device(): lax.all_gather(up_weight, 'sp', axis=0, tiled=True)  84.3 us
    all_gather x1, waiting for transfers between devices, on_device(): lax.all_gather(values, 'sp', axis=0, tiled=True)  39.8 us
    all_gather x1, waiting for transfers between devices, on_device(): lax.all_gather(key_flat, 'sp', axis=0, tiled=True)  38.1 us
    reduce_scatter x1, waiting for transfers between devices, on_device(): lax.psum_scatter(jnp.dot(hidden, down_full, preferred_element_type=jnp.fl...  29.5 us
    all_gather x1, waiting for transfers between devices, on_device(): mixer_in = lax.all_gather(normed, 'tp', axis=0, tiled=True)  18.5 us
    dot_general x4, matrix products, step(): jnp.einsum('cgqk,kcd->cgqd', exp_scores.astype(jnp.bfloat16), value_block...  18.4 us
  transfers between devices with their start and end apart: 7, of which 7 were waited for; matrix products, arithmetic and copies ran while one was open for 3% of the time, Pallas kernels for 0%

commit v1 on v0

--- a/solution.py
+++ b/solution.py
@@ -114,7 +114,12 @@
         lax.all_gather(up_weight, "sp", axis=0, tiled=True),
         preferred_element_type=jnp.float32,
     )
-    down_full = lax.all_gather(down_weight, "sp", axis=1, tiled=True)
+    ring = [down_weight]
+    for hop in range(7):
+        ring.append(lax.ppermute(ring[-1], "sp", [(dev, (dev + 1) % 8) for dev in range(8)]))
+    down_full = jnp.roll(
+        jnp.concatenate(ring[::-1], axis=1), (lax.axis_index("sp") + 1) * ring[0].shape[1], axis=1
+    )
     hidden = (jax.nn.silu(gate_proj) * up_proj).astype(jnp.bfloat16)
     mlp_branch = lax.psum_scatter(
         jnp.dot(hidden, down_full, preferred_element_type=jnp.float32).astype(jnp.bfloat16),

time: 514 us -> 487 us (0.947)
  waiting for transfers between devices: 400 us -> 343 us
  local copies, waits for them, and re-layouts: 11 us -> 32.9 us
  other arithmetic: 13.9 us -> 28 us
  matrix products: 62.7 us -> 56.2 us
    ppermute x0 -> x7, waiting for transfers between devices: none -> 203 us  [on_device(): lax.ppermute(ring[-1], 'sp', [(dev, (dev + 1) % 8) for dev in range(8)])]
    all_gather x1, waiting for transfers between devices: 94.4 us -> 0.01 us  [on_device(): lax.all_gather(gate_weight, 'sp', axis=0, tiled=True)]
    all_gather x1 -> x0, waiting for transfers between devices: 93.2 us -> none  [on_device(): down_full = lax.all_gather(down_weight, 'sp', axis=1, tiled=True)]
    all_gather x1, waiting for transfers between devices: 84.3 us -> 30.9 us  [on_device(): lax.all_gather(up_weight, 'sp', axis=0, tiled=True)]
    unnamed x14 -> x39, local copies, waits for them, and re-layouts: 4.17 us -> 27.1 us
    all_gather x1, waiting for transfers between devices: 18.5 us -> 0.01 us  [on_device(): mixer_in = lax.all_gather(normed, 'tp', axis=0, tiled=True)]
    reduce_sum x4, other arithmetic: 5.55 us -> 19.7 us  [step(): weight_sum = weight_sum * factor + jnp.sum(exp_scores, axis=-1)]
    dot_general x4, matrix products: 18.4 us -> 11.8 us  [step(): jnp.einsum('cgqk,kcd->cgqd', exp_scores.astype(jnp.bfloat16), value_block...]
  transfers between devices with their start and end apart: 7 -> 13, of which waited for: 7 -> 11; matrix products, arithmetic and copies ran while one was open for 3% -> 7% of each run, Pallas kernels for 0% -> 0%
where the time goes in v1:
time: 487 us; the launch traced here: 486 us
  waiting for transfers between devices  343 us (70%)
  matrix products  56.2 us (12%)
  local copies, waits for them, and re-layouts  32.9 us (7%)
  other arithmetic  28 us (6%)
  between operations  13.7 us (3%)
  blocking collectives  11.3 us (2%)
    ppermute x7, waiting for transfers between devices, on_device(): lax.ppermute(ring[-1], 'sp', [(dev, (dev + 1) % 8) for dev in range(8)])  203 us
    all_gather x1, waiting for transfers between devices, on_device(): lax.all_gather(values, 'sp', axis=0, tiled=True)  39.8 us
    all_gather x1, waiting for transfers between devices, on_device(): lax.all_gather(key_flat, 'sp', axis=0, tiled=True)  38.1 us
    all_gather x1, waiting for transfers between devices, on_device(): lax.all_gather(up_weight, 'sp', axis=0, tiled=True)  30.9 us
    reduce_scatter x1, waiting for transfers between devices, on_device(): lax.psum_scatter(jnp.dot(hidden, down_full, preferred_element_type=jnp.fl...  29.5 us
    unnamed x39, local copies, waits for them, and re-layouts  27.1 us
    reduce_sum x4, other arithmetic, step(): weight_sum = weight_sum * factor + jnp.sum(exp_scores, axis=-1)  19.7 us
    dot_general x4, matrix products, step(): jnp.einsum('qcgd,kcd->cgqk', grouped, key_block, preferred_element_type=j...  18 us
  transfers between devices with their start and end apart: 13, of which 11 were waited for; matrix products, arithmetic and copies ran while one was open for 7% of the time, Pallas kernels for 0%

profile of v1, /device:TPU:0, one launch (start us, length us, event | category | flops | bytes accessed | tf_op | source)
XLA Modules:
  0.0 486.3 jit_solution(3447805818143508304)
XLA Ops:
  6.6 1.0 copy.17
  11.3 1.3 copy.18
  13.9 38.1 %all-gather.6.cloned.1.call-done = bf16[4096,128]{0,1:T(8,128)(2,1)} async-done(((bf16[512,128]{0,1:T(8,128)(2,1)}), bf16[4096,128]{0,1:T(8,128)(2,1)}) %all-gather.6.cloned.1.call-update) | async-done | bytes 1048592 | tf_op jit(solution)/shard_map/all_gather | solution.py:61
  52.0 1.6 copy.24
  53.6 39.8 %all-gather.8.cloned.1.call-done = bf16[4096,128]{1,0:T(8,128)(2,1)} async-done(((bf16[512,128]{1,0:T(8,128)(2,1)}), bf16[4096,128]{1,0:T(8,128)(2,1)}) %all-gather.8.cloned.1.call-update) | async-done | bytes 1048592 | tf_op jit(solution)/shard_map/all_gather | solution.py:62
  93.4 52.9 %while.15 = (s32[]{:T(128)}, f32[1,4,512]{2,1,0:T(4,128)S(1)}, f32[1,4,512]{2,1,0:T(4,128)S(1)}, f32[1,4,512,128]{3,2,1,0:T(8,128)S(1)}, bf16[4,1024,1,128]{3,1,...) while((s32[]{:T(128)}, f32[1,4,512]{2,1,0:T(4,128)S(1)}, ...), condition=%wide.region_5.6_spmd.clone, body=%wide.region_2.5_spmd.clone.sunk | while | flops 1091317760 | bytes 61997204 | solution.py:93
  93.4 4.5 bitcast_reduce_fusion.3
  97.9 4.9 %fusion.64 = f32[4,512]{1,0:T(4,128)S(1)} fusion(f32[1024,512,4]{1,0,2:T(8,128)} %get-tuple-element.155, f32[4,512]{1,0:T(4,128)S(1)} %bitcast.99), kind=kLoop, calls=%fused_computation.4.clone.1 | loop fusion | flops 6289408 | bytes 8404992 | tf_op jit(solution)/shard_map/while/body/eval_jaxpr/reduce_sum | solution.py:79
  103.7 2.9 fusion.65
  106.6 4.5 bitcast_reduce_fusion.3
  111.2 4.9 %fusion.64 = f32[4,512]{1,0:T(4,128)S(1)} fusion(f32[1024,512,4]{1,0,2:T(8,128)} %get-tuple-element.155, f32[4,512]{1,0:T(4,128)S(1)} %bitcast.99), kind=kLoop, calls=%fused_computation.4.clone.1 | loop fusion | flops 6289408 | bytes 8404992 | tf_op jit(solution)/shard_map/while/body/eval_jaxpr/reduce_sum | solution.py:79
  116.9 2.9 fusion.65
  119.9 4.5 bitcast_reduce_fusion.3
  124.4 4.9 %fusion.64 = f32[4,512]{1,0:T(4,128)S(1)} fusion(f32[1024,512,4]{1,0,2:T(8,128)} %get-tuple-element.155, f32[4,512]{1,0:T(4,128)S(1)} %bitcast.99), kind=kLoop, calls=%fused_computation.4.clone.1 | loop fusion | flops 6289408 | bytes 8404992 | tf_op jit(solution)/shard_map/while/body/eval_jaxpr/reduce_sum | solution.py:79
  130.1 2.9 fusion.65
  133.1 4.5 bitcast_reduce_fusion.3
  137.6 4.9 %fusion.64 = f32[4,512]{1,0:T(4,128)S(1)} fusion(f32[1024,512,4]{1,0,2:T(8,128)} %get-tuple-element.155, f32[4,512]{1,0:T(4,128)S(1)} %bitcast.99), kind=kLoop, calls=%fused_computation.4.clone.1 | loop fusion | flops 6289408 | bytes 8404992 | tf_op jit(solution)/shard_map/while/body/eval_jaxpr/reduce_sum | solution.py:79
  143.4 2.9 fusion.65
  147.3 11.3 %all_to_all.16 = bf16[4,128,512]{2,1,0:T(8,128)(2,1)S(1)} all-to-all(bf16[4,128,512]{2,1,0:T(8,128)(2,1)S(1)} %convert_element_type.88), channel_id=1, replica_groups=mesh['sp'=8,'tp'=4] {'tp'}, dimensions={0} | all-to-all | bytes 1048576 | tf_op jit(solution)/shard_map/all_to_all | solution.py:100
  158.9 4.8 multiply_reduce_fusion
  164.2 1.0 fusion.34
  167.0 19.7 %collective-permute-done = bf16[1408,256]{1,0:T(8,128)(2,1)S(1)} collective-permute-done((bf16[1408,256]{1,0:T(8,128)(2,1)S(1)}, bf16[1408,256]{1,0:T(8,128)(2,1)S(1)}, u32[]{:S(2)}, u32[]{:S(2)}) %collective-permute-start) | collective-permute-done | bytes 720928 | tf_op jit(solution)/shard_map/ppermute | solution.py:119
  186.7 26.6 %collective-permute-done.1 = bf16[1408,256]{1,0:T(8,128)(2,1)S(1)} collective-permute-done((bf16[1408,256]{1,0:T(8,128)(2,1)S(1)}, bf16[1408,256]{1,0:T(8,128)(2,1)S(1)}, u32[]{:S(2)}, u32[]{:S(2)}) %collective-permute-start.1) | collective-permute-done | bytes 720928 | tf_op jit(solution)/shard_map/ppermute | solution.py:119
  213.2 31.5 %collective-permute-done.2 = bf16[1408,256]{1,0:T(8,128)(2,1)S(1)} collective-permute-done((bf16[1408,256]{1,0:T(8,128)(2,1)S(1)}, bf16[1408,256]{1,0:T(8,128)(2,1)S(1)}, u32[]{:S(2)}, u32[]{:S(2)}) %collective-permute-start.2) | collective-permute-done | bytes 720928 | tf_op jit(solution)/shard_map/ppermute | solution.py:119
  244.7 34.9 %collective-permute-done.3 = bf16[1408,256]{1,0:T(8,128)(2,1)S(1)} collective-permute-done((bf16[1408,256]{1,0:T(8,128)(2,1)S(1)}, bf16[1408,256]{1,0:T(8,128)(2,1)S(1)}, u32[]{:S(2)}, u32[]{:S(2)}) %collective-permute-start.3) | collective-permute-done | bytes 720928 | tf_op jit(solution)/shard_map/ppermute | solution.py:119
  280.6 35.1 %collective-permute-done.4 = bf16[1408,256]{1,0:T(8,128)(2,1)S(1)} collective-permute-done((bf16[1408,256]{1,0:T(8,128)(2,1)S(1)}, bf16[1408,256]{1,0:T(8,128)(2,1)S(1)}, u32[]{:S(2)}, u32[]{:S(2)}) %collective-permute-start.4) | collective-permute-done | bytes 720928 | tf_op jit(solution)/shard_map/ppermute | solution.py:119
  316.5 25.7 %collective-permute-done.5 = bf16[1408,256]{1,0:T(8,128)(2,1)} collective-permute-done((bf16[1408,256]{1,0:T(8,128)(2,1)S(1)}, bf16[1408,256]{1,0:T(8,128)(2,1)}, u32[]{:S(2)}, u32[]{:S(2)}) %collective-permute-start.5) | collective-permute-done | bytes 720928 | tf_op jit(solution)/shard_map/ppermute | solution.py:119
  342.2 29.6 %collective-permute-done.6 = bf16[1408,256]{1,0:T(8,128)(2,1)} collective-permute-done((bf16[1408,256]{1,0:T(8,128)(2,1)}, bf16[1408,256]{1,0:T(8,128)(2,1)}, u32[]{:S(2)}, u32[]{:S(2)}) %collective-permute-start.6) | collective-permute-done | bytes 720928 | tf_op jit(solution)/shard_map/ppermute | solution.py:119
  371.8 2.1 constant_dynamic-update-slice_fusion.15
  373.9 2.1 constant_dynamic-update-slice_fusion.14
  376.0 2.1 constant_dynamic-update-slice_fusion.13
  378.0 2.0 constant_dynamic-update-slice_fusion.12
  380.1 1.0 constant_dynamic-update-slice_fusion.11
  381.0 1.0 constant_dynamic-update-slice_fusion.10
  382.0 1.0 constant_dynamic-update-slice_fusion.9
  384.0 2.1 constant_dynamic-update-slice_fusion.7
  386.1 2.1 constant_dynamic-update-slice_fusion.6
  388.2 1.0 constant_dynamic-update-slice_fusion.5
  389.1 1.0 constant_dynamic-update-slice_fusion.4
  391.1 1.0 constant_dynamic-update-slice_fusion.2
  392.1 1.0 constant_dynamic-update-slice_fusion.1
  393.0 1.0 constant_dynamic-update-slice_fusion
  394.0 8.4 %fusion.49 = f32[512,1408]{1,0:T(8,128)} fusion(bf16[512,2048]{1,0:T(8,128)(2,1)} %all-gather.10.cloned.1.call-done, bf16[2048,1408]{1,0:T(8,128)(2,1)} %all-gather.12.cloned.1.call-done), kind=kOutput, calls=%fused_computation.100 | convolution fusion | flops 2952790016 | bytes 10747904 | tf_op jit(solution)/shard_map/dot_general | solution.py:107
  402.4 30.9 %all-gather.14.cloned.1.call-done = bf16[2048,1408]{1,0:T(8,128)(2,1)} async-done(((bf16[256,1408]{1,0:T(8,128)(2,1)}), bf16[2048,1408]{1,0:T(8,128)(2,1)}) %all-gather.14.cloned.1.call-update) | async-done | bytes 5767184 | tf_op jit(solution)/shard_map/all_gather | solution.py:114
  433.3 13.2 %fusion.27 = bf16[512,2048]{1,0:T(8,128)(2,1)} fusion(bf16[1408,4096]{1,0:T(8,128)(2,1)} %constant_dynamic-update-slice_fusion, s32[]{:T(128)S(6)} %select_n.48, bf16[512,2048]{1,0:T(8,128)(2,1)S(1)} %copy-done.10, bf16[2048,1408]{1,0:T(8,128)(2,1)} %all-gather.14.cloned.1.call-done, f32[512,1408]{1,0:T(8,128)} %fusion.49), kind=kOutput, calls=%fused_computation.30 | convolution fusion | flops 5910953984 | bytes 18612228 | tf_op jit(solution)/shard_map/dot_general | solution.py:125
  446.6 29.5 %reduce-scatter.2.cloned.1.call-done = bf16[128,2048]{1,0:T(8,128)(2,1)} async-done(((bf16[512,2048]{1,0:T(8,128)(2,1)}), bf16[128,2048]{1,0:T(8,128)(2,1)}) %reduce-scatter.2.cloned.1.call-update) | async-done | bytes 524304 | tf_op jit(solution)/shard_map/reduce_scatter | solution.py:124
  476.1 1.2 fusion.30
  477.3 2.1 fusion.35
  (90 shorter events, 15.4 us)
Async XLA Ops:
  6.5 45.4 %all-gather.6.cloned.1.call-start = ((), (), s32[]{:S(2)}) async-start(), calls=%async_computation.2 | async-start | bytes 1179648 | tf_op jit(solution)/shard_map/all_gather | solution.py:61
  9.7 83.7 %all-gather.8.cloned.1.call-start = ((), (), s32[]{:S(2)}) async-start(), calls=%async_computation.3 | async-start | bytes 1179648 | tf_op jit(solution)/shard_map/all_gather | solution.py:62
  10.4 383.6 %all-gather.10.cloned.1.call-start = ((), (), s32[]{:S(2)}) async-start(), calls=%async_computation.4 | async-start | bytes 2621440 | tf_op jit(solution)/shard_map/all_gather | solution.py:106
  97.9 5.8 %copy-start = (f32[1024,512,4]{1,0,2:T(8,128)S(1)}, f32[1024,512,4]{1,0,2:T(8,128)}, u32[]{:S(2)}) copy-start(f32[1024,512,4]{1,0,2:T(8,128)} %get-tuple-element.155) | copy-start | bytes 25165828 | tf_op jit(solution)/shard_map/while
  111.1 5.8 %copy-start = (f32[1024,512,4]{1,0,2:T(8,128)S(1)}, f32[1024,512,4]{1,0,2:T(8,128)}, u32[]{:S(2)}) copy-start(f32[1024,512,4]{1,0,2:T(8,128)} %get-tuple-element.155) | copy-start | bytes 25165828 | tf_op jit(solution)/shard_map/while
  124.4 5.8 %copy-start = (f32[1024,512,4]{1,0,2:T(8,128)S(1)}, f32[1024,512,4]{1,0,2:T(8,128)}, u32[]{:S(2)}) copy-start(f32[1024,512,4]{1,0,2:T(8,128)} %get-tuple-element.155) | copy-start | bytes 25165828 | tf_op jit(solution)/shard_map/while
  137.6 5.8 %copy-start = (f32[1024,512,4]{1,0,2:T(8,128)S(1)}, f32[1024,512,4]{1,0,2:T(8,128)}, u32[]{:S(2)}) copy-start(f32[1024,512,4]{1,0,2:T(8,128)} %get-tuple-element.155) | copy-start | bytes 25165828 | tf_op jit(solution)/shard_map/while
  158.6 5.1 %copy-start.6 = (bf16[128,2048]{1,0:T(8,128)(2,1)S(1)}, bf16[128,2048]{1,0:T(8,128)(2,1)}, u32[]{:S(2)}) copy-start(bf16[128,2048]{1,0:T(8,128)(2,1)} %param.22) | copy-start | bytes 1572868
  158.6 5.1 %copy-start.7 = (f32[2048]{0:T(1024)S(1)}, f32[2048]{0:T(1024)}, u32[]{:S(2)}) copy-start(f32[2048]{0:T(1024)} %param.21) | copy-start | bytes 24580
  158.9 5.3 %copy-start.8 = (f32[2048]{0:T(1024)S(1)}, f32[2048]{0:T(1024)}, u32[]{:S(2)}) copy-start(f32[2048]{0:T(1024)} %param.23) | copy-start | bytes 24580
  158.9 7.5 %copy-start.1 = (bf16[1408,256]{1,0:T(8,128)(2,1)S(1)}, bf16[1408,256]{1,0:T(8,128)(2,1)}, u32[]{:S(2)}) copy-start(bf16[1408,256]{1,0:T(8,128)(2,1)} %param.26) | copy-start | bytes 2162692
  165.2 228.8 %all-gather.12.cloned.1.call-start = ((), (), s32[]{:S(2)}) async-start(), calls=%async_computation.5 | async-start | bytes 6488064 | tf_op jit(solution)/shard_map/all_gather | solution.py:109
  165.8 267.6 %all-gather.14.cloned.1.call-start = ((), (), s32[]{:S(2)}) async-start(), calls=%async_computation.6 | async-start | bytes 6488064 | tf_op jit(solution)/shard_map/all_gather | solution.py:114
  166.4 309.7 %reduce-scatter.2.cloned.1.call-start = ((), (), s32[]{:S(2)}) async-start(), calls=%async_computation.7 | async-start | bytes 2621440 | tf_op jit(solution)/shard_map/reduce_scatter | solution.py:124
  166.4 20.3 %collective-permute-start = (bf16[1408,256]{1,0:T(8,128)(2,1)S(1)}, bf16[1408,256]{1,0:T(8,128)(2,1)S(1)}, u32[]{:S(2)}, u32[]{:S(2)}) collective-permute-start(bf16[1408,256]{1,0:T(8,128)(2,1)S(1)} %copy-done.1), channel_id=1, source_target_pairs={{0,4},{4,8},{8,12},{12,16},{16,20},{20,24},{24,28},{28,0},{1,5},{5... | collective-permute-start | bytes 2162696 | tf_op jit(solution)/shard_map/ppermute | solution.py:119
  186.7 26.6 %collective-permute-start.1 = (bf16[1408,256]{1,0:T(8,128)(2,1)S(1)}, bf16[1408,256]{1,0:T(8,128)(2,1)S(1)}, u32[]{:S(2)}, u32[]{:S(2)}) collective-permute-start(bf16[1408,256]{1,0:T(8,128)(2,1)S(1)} %collective-permute-done), channel_id=1, source_target_pairs={{0,4},{4,8},{8,12},{12,16},{16,20},{20,24},{24,28},{28,0},{1,5},{5... | collective-permute-start | bytes 2162696 | tf_op jit(solution)/shard_map/ppermute | solution.py:119
  213.2 31.5 %collective-permute-start.2 = (bf16[1408,256]{1,0:T(8,128)(2,1)S(1)}, bf16[1408,256]{1,0:T(8,128)(2,1)S(1)}, u32[]{:S(2)}, u32[]{:S(2)}) collective-permute-start(bf16[1408,256]{1,0:T(8,128)(2,1)S(1)} %collective-permute-done.1), channel_id=1, source_target_pairs={{0,4},{4,8},{8,12},{12,16},{16,20},{20,24},{24,28},{28,0},{1,5},{5... | collective-permute-start | bytes 2162696 | tf_op jit(solution)/shard_map/ppermute | solution.py:119
  244.7 34.9 %collective-permute-start.3 = (bf16[1408,256]{1,0:T(8,128)(2,1)S(1)}, bf16[1408,256]{1,0:T(8,128)(2,1)S(1)}, u32[]{:S(2)}, u32[]{:S(2)}) collective-permute-start(bf16[1408,256]{1,0:T(8,128)(2,1)S(1)} %collective-permute-done.2), channel_id=1, source_target_pairs={{0,4},{4,8},{8,12},{12,16},{16,20},{20,24},{24,28},{28,0},{1,5},{5... | collective-permute-start | bytes 2162696 | tf_op jit(solution)/shard_map/ppermute | solution.py:119
  279.7 0.9 copy-start.2
  280.6 35.1 %collective-permute-start.4 = (bf16[1408,256]{1,0:T(8,128)(2,1)S(1)}, bf16[1408,256]{1,0:T(8,128)(2,1)S(1)}, u32[]{:S(2)}, u32[]{:S(2)}) collective-permute-start(bf16[1408,256]{1,0:T(8,128)(2,1)S(1)} %collective-permute-done.3), channel_id=1, source_target_pairs={{0,4},{4,8},{8,12},{12,16},{16,20},{20,24},{24,28},{28,0},{1,5},{5... | collective-permute-start | bytes 2162696 | tf_op jit(solution)/shard_map/ppermute | solution.py:119
  315.6 0.8 copy-start.4
  316.5 25.7 %collective-permute-start.5 = (bf16[1408,256]{1,0:T(8,128)(2,1)S(1)}, bf16[1408,256]{1,0:T(8,128)(2,1)}, u32[]{:S(2)}, u32[]{:S(2)}) collective-permute-start(bf16[1408,256]{1,0:T(8,128)(2,1)S(1)} %collective-permute-done.4), channel_id=1, source_target_pairs={{0,4},{4,8},{8,12},{12,16},{16,20},{20,24},{24,28},{28,0},{1,5},{5... | collective-permute-start | bytes 2162696 | tf_op jit(solution)/shard_map/ppermute | solution.py:119
  342.1 29.7 %collective-permute-start.6 = (bf16[1408,256]{1,0:T(8,128)(2,1)}, bf16[1408,256]{1,0:T(8,128)(2,1)}, u32[]{:S(2)}, u32[]{:S(2)}) collective-permute-start(bf16[1408,256]{1,0:T(8,128)(2,1)} %collective-permute-done.5), channel_id=1, source_target_pairs={{0,4},{4,8},{8,12},{12,16},{16,20},{20,24},{24,28},{28,0},{1,5},{5... | collective-permute-start | bytes 2162696 | tf_op jit(solution)/shard_map/ppermute | solution.py:119
  342.2 46.0 %copy-start.5 = (bf16[1408,256]{1,0:T(8,128)(2,1)S(1)}, bf16[1408,256]{1,0:T(8,128)(2,1)}, u32[]{:S(2)}) copy-start(bf16[1408,256]{1,0:T(8,128)(2,1)} %copy-done.4) | copy-start | bytes 2162692
  342.2 47.0 %copy-start.3 = (bf16[1408,256]{1,0:T(8,128)(2,1)S(1)}, bf16[1408,256]{1,0:T(8,128)(2,1)}, u32[]{:S(2)}) copy-start(bf16[1408,256]{1,0:T(8,128)(2,1)} %copy-done.2) | copy-start | bytes 2162692
  394.0 39.3 %copy-start.10 = (bf16[512,2048]{1,0:T(8,128)(2,1)S(1)}, bf16[512,2048]{1,0:T(8,128)(2,1)}, u32[]{:S(2)}) copy-start(bf16[512,2048]{1,0:T(8,128)(2,1)} %all-gather.10.cloned.1.call-done) | copy-start | bytes 6291460
  402.4 74.9 %copy-start.9 = (f32[2048]{0:T(1024)S(1)}, f32[2048]{0:T(1024)}, u32[]{:S(2)}) copy-start(f32[2048]{0:T(1024)} %param.27) | copy-start | bytes 24580
Sparse Core Ops, SparseCore 0:
  9.8 42.1 all-gather.5
  54.1 39.2 all-gather.7
  165.3 20.3 all-gather.9
  187.8 134.9 all-gather.11
  324.8 108.4 all-gather.13
  446.7 29.3 reduce-scatter.1
